TPU v7x, 32 devices: a whole 2x2x4 slice. The times are simulated.
32 devices in a mesh: sp: 8 (over z, x), tp: 4 (over y, core).
Axes of the slice: x: 2, y: 2, z: 4, core: 2. Of those that a mesh axis runs over, the one named last changes fastest.
Arguments:
- layer_input: bfloat16 [4, 2048, 2048], P(None, ('sp', 'tp')), as said below
- key_weight: bfloat16 [2048, 384], replicated, may hold values from -0.125 to 0.125
- value_weight: bfloat16 [2048, 384], replicated, may hold values from -0.125 to 0.125
- queries: bfloat16 [24, 5, 64], P('sp'), may hold values from -6 to 6
- head_bias: float32 [6, 5], replicated, as said below
Outputs:
- stored: bfloat16 [24, 8, 256, 128], P('sp', None, 'tp')
- first_read: bfloat16 [24, 320], P('sp')
Inputs may be any that keep to these rules, and one draw needn't show every extreme that they name: `layer_input`: entries lie between -12.5 and 12.5. `head_bias`: entries lie between -1 minus the natural logarithm of 2048 and -3.
All inputs are finite; a program needn't handle non-finite values.
Results may differ from a plain program's by a relative error of at most 0.01.
Values may be sent and summed in bfloat16 or wider, within the bound.
A program may use at most 64 MiB of HBM per device.

v0:
```python
import math
import jax
import jax.numpy as jnp
from jax import lax
from jax.sharding import PartitionSpec as P

HD = 64
KVH = 6
GROUP = 5
EPS_NORM = 0.0001


def head_norm(summed):
    squares = jnp.mean(summed * summed, axis=-1, keepdims=True)
    return summed * lax.rsqrt(squares + EPS_NORM)


def shift_table(pair_ids, head_bias):
    heads_range = jnp.arange(KVH, dtype=jnp.int32)
    picker = (pair_ids[:, None] % KVH == heads_range[None, :]).astype(jnp.float32)
    return jnp.dot(picker, head_bias, precision=lax.Precision.HIGHEST)


def per_device(layer_input, key_weight, value_weight, queries, head_bias):
    seq_count, positions, model_width = layer_input.shape
    tokens_flat = layer_input.reshape(seq_count * positions, model_width)
    key_rows = (
        jnp.dot(tokens_flat, key_weight, preferred_element_type=jnp.float32)
        .astype(jnp.bfloat16)
        .reshape(seq_count, positions, KVH, HD)
    )
    value_rows = (
        jnp.dot(tokens_flat, value_weight, preferred_element_type=jnp.float32)
        .astype(jnp.bfloat16)
        .reshape(seq_count, positions, KVH, HD)
    )
    kv_rows = (
        jnp.concatenate([key_rows, value_rows], axis=-1)
        .transpose(0, 2, 1, 3)
        .reshape(seq_count * KVH, 1, positions, 2 * HD)
    )
    stored = lax.all_to_all(kv_rows, "sp", split_axis=0, concat_axis=1, tiled=True)
    score_scale = 1.0 / math.sqrt(HD)
    local_pairs = queries.shape[0]
    pair_ids = lax.axis_index("sp") * local_pairs + jnp.arange(local_pairs, dtype=jnp.int32)
    head_shift = shift_table(pair_ids, head_bias)
    scores = (
        jnp.einsum("pgc,pbtc->pgbt", queries, stored[..., :HD], preferred_element_type=jnp.float32)
        * score_scale
        + head_shift[:, :, None, None]
    )
    keep_log = jax.nn.log_sigmoid(-scores)
    totals = jnp.sum(keep_log, axis=3)
    gathered = lax.all_gather(totals[None], "tp", axis=0, tiled=True)
    later_mask = (jnp.arange(gathered.shape[0], dtype=jnp.int32) > lax.axis_index("tp")).astype(
        jnp.float32
    )
    later_inside = jnp.sum(gathered * later_mask[:, None, None, None], axis=0)
    block_sums = jnp.sum(gathered, axis=0)
    later_blocks = lax.cumsum(block_sums, axis=2, reverse=True) - block_sums
    suffix_log = (
        lax.cumsum(keep_log, axis=3, reverse=True)
        - keep_log
        + (later_inside + later_blocks)[..., None]
    )
    weights = jnp.exp(jax.nn.log_sigmoid(scores) + suffix_log).astype(jnp.bfloat16)
    partial_value = jnp.einsum(
        "pgbt,pbtc->pgc", weights, stored[..., HD:], preferred_element_type=jnp.float32
    )
    summed = lax.psum(partial_value, "tp")
    first_read = head_norm(summed).reshape(local_pairs, GROUP * HD).astype(jnp.bfloat16)
    return (stored, first_read)


def solution(mesh):
    in_specs = (P(None, ("sp", "tp"), None), P(), P(), P("sp", None, None), P())
    out_specs = (P("sp", None, "tp", None), P("sp", None))
    return jax.shard_map(
        per_device, mesh=mesh, in_specs=in_specs, out_specs=out_specs, check_vma=False
    )
```

profile of v0, /device:TPU:0, one launch (start us, length us, event | category | flops | bytes accessed | tf_op | source)
XLA Modules:
  0.0 53.3 jit_solution(13283465844717739790)
XLA Ops:
  0.6 0.0 copy-start
  0.6 1.4 %copy-done = bf16[2048,384]{1,0:T(8,128)(2,1)S(1)} copy-done((bf16[2048,384]{1,0:T(8,128)(2,1)S(1)}, bf16[2048,384]{1,0:T(8,128)(2,1)}, u32[]{:S(2)}) %copy-start) | copy-done | bytes 1572888
  2.0 0.0 copy-start.2
  2.0 2.0 %convolution_convert_fusion.1 = bf16[256,384]{1,0:T(8,128)(2,1)S(1)} fusion(bf16[256,2048]{1,0:T(8,128)(2,1)} %bitcast.33, bf16[2048,384]{1,0:T(8,128)(2,1)S(1)} %copy-done), kind=kOutput, calls=%fused_computation.1 | convolution fusion | flops 402751488 | bytes 2818048 | tf_op jit(solution)/shard_map/dot_general | solution.py:28
  4.1 0.1 copy.26
  4.2 0.2 reshape.69
  4.4 0.0 copy-done.2
  4.4 2.1 %convolution_convert_fusion = bf16[256,384]{1,0:T(8,128)(2,1)S(1)} fusion(bf16[256,2048]{1,0:T(8,128)(2,1)S(1)} %bitcast.34, bf16[2048,384]{1,0:T(8,128)(2,1)} %param.7), kind=kOutput, calls=%fused_computation | convolution fusion | flops 402751488 | bytes 2818048 | tf_op jit(solution)/shard_map/dot_general | solution.py:33
  6.6 0.1 copy.27
  6.7 0.2 reshape.70
  6.9 0.0 copy-start.4
  6.9 0.6 %maximum_bitcast_fusion = bf16[4,6,64,128]{2,0,3,1:T(4,128)(2,1)S(1)} fusion(bf16[4,64,6,64]{1,0,3,2:T(4,128)(2,1)S(1)} %reshape.70, bf16[4,64,6,64]{1,0,3,2:T(4,128)(2,1)S(1)} %reshape.69), kind=kLoop, calls=%fused_computation.6 | loop fusion | flops 196608 | bytes 786432 | tf_op jit(solution)/shard_map/transpose | solution.py:39
  7.6 0.0 copy-start.3
  7.6 1.2 %copy.28 = bf16[4,6,64,128]{3,2,1,0:T(8,128)(2,1)} copy(bf16[4,6,64,128]{2,0,3,1:T(4,128)(2,1)S(1)} %maximum_bitcast_fusion) | data formatting | bytes 786432 | tf_op jit(solution)/shard_map/transpose | solution.py:39
  8.7 7.3 %all-to-all-start = ((bf16[24,1,64,128]{3,2,1,0:T(8,128)(2,1)}), bf16[24,1,64,128]{3,2,1,0:T(8,128)(2,1)S(1)}, u32[]{:S(2)}, u32[]{:S(2)}) async-start(bf16[24,1,64,128]{3,2,1,0:T(8,128)(2,1)} %bitcast.3), calls=%async_computation | async-start | bytes 786432 | tf_op jit(solution)/shard_map/all_to_all | solution.py:42
  16.0 0.0 copy-done.4
  16.1 0.2 fusion.15
  16.2 11.5 %all-to-all-done = bf16[24,1,64,128]{3,2,1,0:T(8,128)(2,1)S(1)} async-done(((bf16[24,1,64,128]{3,2,1,0:T(8,128)(2,1)}), bf16[24,1,64,128]{3,2,1,0:T(8,128)(2,1)S(1)}, u32[]{:S(2)}, u32[]{:S(2)}) %all-to-all-start) | async-done | bytes 393248 | tf_op jit(solution)/shard_map/all_to_all | solution.py:42
  27.7 0.0 copy-start.1
  27.7 0.0 copy-done.3
  27.8 0.5 fusion.9
  28.3 0.1 copy.34
  28.4 5.2 %all-gather = f32[12,5,8]{2,1,0:T(8,128)S(1)} all-gather(f32[3,5,8]{2,1,0:T(8,128)S(1)} %copy.34), channel_id=2, replica_groups=mesh['sp'=8,'tp'=4] {'tp'}, dimensions={0}, use_global_device_ids=true | all-gather | bytes 2400 | tf_op jit(solution)/shard_map/all_gather | solution.py:54
  33.6 0.1 fusion.19
  33.7 0.5 reduce_window_sum.21
  34.2 0.1 copy.35
  34.3 6.4 %reduce_window_sum.20 = f32[3,5,8,64]{3,2,1,0:T(8,128)S(1)} reduce-window(f32[3,5,8,64]{3,2,1,0:T(8,128)S(1)} %copy.32, f32[]{:T(128)} %constant.36.clone.1), window={size=1x1x1x64 pad=0_0x0_0x0_0x0_63}, to_apply=%region_0.1 | reduce-window | flops 483840 | bytes 61444 | tf_op jit(solution)/shard_map/per_device/reduce_window_sum | solution.py:62
  40.7 0.4 convolution_bitcast_fusion
  41.1 11.4 %psum.7 = f32[3,5,64]{2,1,0:T(8,128)S(1)} all-reduce(f32[3,5,64]{2,1,0:T(8,128)S(1)} %convolution_bitcast_fusion), channel_id=1, replica_groups=mesh['sp'=8,'tp'=4] {'tp'}, use_global_device_ids=true, to_apply=%region_5.6 | all-reduce | flops 960 | bytes 7680 | tf_op jit(solution)/shard_map/psum | solution.py:70
  52.5 0.1 multiply_reduce_fusion.1
  52.6 0.1 multiply_convert_fusion
  52.7 0.7 %convert_element_type.28 = bf16[3,320]{1,0:T(4,128)(2,1)} reshape(bf16[3,5,64]{2,1,0:T(8,128)(2,1)S(1)} %multiply_convert_fusion) | data formatting | bytes 3840 | tf_op jit(solution)/shard_map/convert_element_type | solution.py:71
  53.3 0.0 copy-done.1
  (7 shorter events, 0.1 us)
Async XLA Ops:
  0.6 1.4 %copy-start = (bf16[2048,384]{1,0:T(8,128)(2,1)S(1)}, bf16[2048,384]{1,0:T(8,128)(2,1)}, u32[]{:S(2)}) copy-start(bf16[2048,384]{1,0:T(8,128)(2,1)} %param.6) | copy-start | bytes 4718596
  2.0 2.4 %copy-start.2 = (bf16[4,64,2048]{2,1,0:T(8,128)(2,1)S(1)}, bf16[4,64,2048]{2,1,0:T(8,128)(2,1)}, u32[]{:S(2)}) copy-start(bf16[4,64,2048]{2,1,0:T(8,128)(2,1)} %param.5) | copy-start | bytes 3145732
  6.9 9.1 %copy-start.4 = (f32[6,5]{1,0:T(8,128)S(1)}, f32[6,5]{1,0:T(8,128)}, u32[]{:S(2)}) copy-start(f32[6,5]{1,0:T(8,128)} %param.9) | copy-start | bytes 364
  7.6 20.2 %copy-start.3 = (bf16[3,5,64]{2,0,1:T(4,128)(2,1)S(1)}, bf16[3,5,64]{2,0,1:T(4,128)(2,1)}, u32[]{:S(2)}) copy-start(bf16[3,5,64]{2,0,1:T(4,128)(2,1)} %param.8) | copy-start | bytes 5764
  8.7 19.0 %all-to-all-start = ((bf16[24,1,64,128]{3,2,1,0:T(8,128)(2,1)}), bf16[24,1,64,128]{3,2,1,0:T(8,128)(2,1)S(1)}, u32[]{:S(2)}, u32[]{:S(2)}) async-start(bf16[24,1,64,128]{3,2,1,0:T(8,128)(2,1)} %bitcast.3), calls=%async_computation | async-start | bytes 786432 | tf_op jit(solution)/shard_map/all_to_all | solution.py:42
  27.7 25.6 %copy-start.1 = (bf16[8,3,1,64,128]{4,3,0,1,2:T(8,128)(2,1)}, bf16[8,3,1,64,128]{4,3,0,1,2:T(8,128)(2,1)S(1)}, u32[]{:S(2)}) copy-start(bf16[8,3,1,64,128]{4,3,0,1,2:T(8,128)(2,1)S(1)} %copy.51) | copy-start | bytes 1179652
where the time goes:
time: 53.7 us; the launch traced here: 53.3 us
  blocking collectives  16.6 us (31%)
  waiting for transfers between devices  11.5 us (21%)
  other arithmetic  7.8 us (15%)
  starting transfers between devices  7.28 us (14%)
  matrix products  5.23 us (10%)
  local copies, waits for them, and re-layouts  4.2 us (8%)
  between operations  0.75 us (1%)
    all_to_all x1, waiting for transfers between devices, per_device(): lax.all_to_all(kv_rows, 'sp', split_axis=0, concat_axis=1, tiled=True)  11.5 us
    psum x1, blocking collectives, per_device(): summed = lax.psum(partial_value, 'tp')  11.4 us
    all_to_all x1, starting transfers between devices, per_device(): lax.all_to_all(kv_rows, 'sp', split_axis=0, concat_axis=1, tiled=True)  7.28 us
    another operation x1, other arithmetic, per_device(): lax.cumsum(keep_log, axis=3, reverse=True) - keep_log  6.41 us
    all_gather x1, blocking collectives, per_device(): gathered = lax.all_gather(totals[None], 'tp', axis=0, tiled=True)  5.21 us
    dot_general x1, matrix products, per_device(): jnp.dot(tokens_flat, value_weight, preferred_element_type=jnp.float32)  2.12 us
    dot_general x1, matrix products, per_device(): jnp.dot(tokens_flat, key_weight, preferred_element_type=jnp.float32)  2.02 us
    unnamed x10, local copies, waits for them, and re-layouts  1.43 us
  transfers between devices with their start and end apart: 1, of which 1 were waited for; matrix products, arithmetic and copies ran while one was open for 0% of the time, Pallas kernels for 0%

commit v1 on v0

--- a/solution.py
+++ b/solution.py
@@ -67,7 +67,8 @@
     partial_value = jnp.einsum(
         "pgbt,pbtc->pgc", weights, stored[..., HD:], preferred_element_type=jnp.float32
     )
-    summed = lax.psum(partial_value, "tp")
+    terms = lax.all_gather(partial_value, "tp")
+    summed = jnp.sum(terms, axis=0)
     first_read = head_norm(summed).reshape(local_pairs, GROUP * HD).astype(jnp.bfloat16)
     return (stored, first_read)
 

time: 53.7 us -> 47.5 us (0.88)
  blocking collectives: 16.6 us -> 10.4 us
    psum x1 -> x0, blocking collectives: 11.4 us -> none  [per_device(): summed = lax.psum(partial_value, 'tp')]
    all_gather x0 -> x1, blocking collectives: none -> 5.21 us  [per_device(): terms = lax.all_gather(partial_value, 'tp')]
where the time goes in v1:
time: 47.5 us; the launch traced here: 47.2 us
  waiting for transfers between devices  11.5 us (24%)
  blocking collectives  10.4 us (22%)
  other arithmetic  7.81 us (16%)
  starting transfers between devices  7.28 us (15%)
  matrix products  5.23 us (11%)
  local copies, waits for them, and re-layouts  4.2 us (9%)
  between operations  0.76 us (2%)
    all_to_all x1, waiting for transfers between devices, per_device(): lax.all_to_all(kv_rows, 'sp', split_axis=0, concat_axis=1, tiled=True)  11.5 us
    all_to_all x1, starting transfers between devices, per_device(): lax.all_to_all(kv_rows, 'sp', split_axis=0, concat_axis=1, tiled=True)  7.28 us
    another operation x1, other arithmetic, per_device(): lax.cumsum(keep_log, axis=3, reverse=True) - keep_log  6.41 us
    all_gather x1, blocking collectives, per_device(): terms = lax.all_gather(partial_value, 'tp')  5.21 us
    all_gather x1, blocking collectives, per_device(): gathered = lax.all_gather(totals[None], 'tp', axis=0, tiled=True)  5.21 us
    dot_general x1, matrix products, per_device(): jnp.dot(tokens_flat, value_weight, preferred_element_type=jnp.float32)  2.12 us
    dot_general x1, matrix products, per_device(): jnp.dot(tokens_flat, key_weight, preferred_element_type=jnp.float32)  2.02 us
    unnamed x10, local copies, waits for them, and re-layouts  1.43 us
  transfers between devices with their start and end apart: 1, of which 1 were waited for; matrix products, arithmetic and copies ran while one was open for 0% of the time, Pallas kernels for 0%

profile of v1, /device:TPU:0, one launch (start us, length us, event | category | flops | bytes accessed | tf_op | source)
XLA Modules:
  0.0 47.2 jit_solution(7443517885763475087)
XLA Ops:
  0.6 0.0 copy-start
  0.6 1.4 %copy-done = bf16[2048,384]{1,0:T(8,128)(2,1)S(1)} copy-done((bf16[2048,384]{1,0:T(8,128)(2,1)S(1)}, bf16[2048,384]{1,0:T(8,128)(2,1)}, u32[]{:S(2)}) %copy-start) | copy-done | bytes 1572888
  2.0 0.0 copy-start.2
  2.0 2.0 %convolution_convert_fusion.1 = bf16[256,384]{1,0:T(8,128)(2,1)S(1)} fusion(bf16[256,2048]{1,0:T(8,128)(2,1)} %bitcast.35, bf16[2048,384]{1,0:T(8,128)(2,1)S(1)} %copy-done), kind=kOutput, calls=%fused_computation.1 | convolution fusion | flops 402751488 | bytes 2818048 | tf_op jit(solution)/shard_map/dot_general | solution.py:28
  4.1 0.1 copy.26
  4.2 0.2 reshape.72
  4.4 0.0 copy-done.2
  4.4 2.1 %convolution_convert_fusion = bf16[256,384]{1,0:T(8,128)(2,1)S(1)} fusion(bf16[256,2048]{1,0:T(8,128)(2,1)S(1)} %bitcast.36, bf16[2048,384]{1,0:T(8,128)(2,1)} %param.7), kind=kOutput, calls=%fused_computation | convolution fusion | flops 402751488 | bytes 2818048 | tf_op jit(solution)/shard_map/dot_general | solution.py:33
  6.6 0.1 copy.27
  6.7 0.2 reshape.73
  6.9 0.0 copy-start.4
  6.9 0.6 %maximum_bitcast_fusion = bf16[4,6,64,128]{2,0,3,1:T(4,128)(2,1)S(1)} fusion(bf16[4,64,6,64]{1,0,3,2:T(4,128)(2,1)S(1)} %reshape.73, bf16[4,64,6,64]{1,0,3,2:T(4,128)(2,1)S(1)} %reshape.72), kind=kLoop, calls=%fused_computation.6 | loop fusion | flops 196608 | bytes 786432 | tf_op jit(solution)/shard_map/transpose | solution.py:39
  7.6 0.0 copy-start.3
  7.6 1.2 %copy.28 = bf16[4,6,64,128]{3,2,1,0:T(8,128)(2,1)} copy(bf16[4,6,64,128]{2,0,3,1:T(4,128)(2,1)S(1)} %maximum_bitcast_fusion) | data formatting | bytes 786432 | tf_op jit(solution)/shard_map/transpose | solution.py:39
  8.7 7.3 %all-to-all-start = ((bf16[24,1,64,128]{3,2,1,0:T(8,128)(2,1)}), bf16[24,1,64,128]{3,2,1,0:T(8,128)(2,1)S(1)}, u32[]{:S(2)}, u32[]{:S(2)}) async-start(bf16[24,1,64,128]{3,2,1,0:T(8,128)(2,1)} %bitcast.3), calls=%async_computation | async-start | bytes 786432 | tf_op jit(solution)/shard_map/all_to_all | solution.py:42
  16.0 0.0 copy-done.4
  16.1 0.2 fusion.15
  16.2 11.5 %all-to-all-done = bf16[24,1,64,128]{3,2,1,0:T(8,128)(2,1)S(1)} async-done(((bf16[24,1,64,128]{3,2,1,0:T(8,128)(2,1)}), bf16[24,1,64,128]{3,2,1,0:T(8,128)(2,1)S(1)}, u32[]{:S(2)}, u32[]{:S(2)}) %all-to-all-start) | async-done | bytes 393248 | tf_op jit(solution)/shard_map/all_to_all | solution.py:42
  27.7 0.0 copy-start.1
  27.7 0.0 copy-done.3
  27.8 0.5 %fusion.9 = (f32[3,5,8]{1,2,0:T(8,128)S(1)}, f32[3,5,8,64]{3,1,2,0:T(8,128)S(1)}, f32[3,5,8,64]{3,1,2,0:T(8,128)S(1)}) fusion(f32[3,5]{1,0:T(4,128)S(1)} %fusion.15, bf16[3,5,64,1]{2,0,1,3:T(4,128)(2,1)S(1)} %bitcast.37, bf16[3,8,64,128]{3,2,1,0:T(8,128)(2,1)S(1)} %bitcast.30), kind=kOutput, calls=%fused_computation.18 | convolution fusion | flops 1059720 | bytes 457116 | tf_op jit(solution)/shard_map/pgc,pbtc->pgbt/dot_general | solution.py:48
  28.3 0.1 copy.34
  28.4 5.2 %all-gather = f32[12,5,8]{2,1,0:T(8,128)S(1)} all-gather(f32[3,5,8]{2,1,0:T(8,128)S(1)} %copy.34), channel_id=2, replica_groups=mesh['sp'=8,'tp'=4] {'tp'}, dimensions={0}, use_global_device_ids=true | all-gather | bytes 2400 | tf_op jit(solution)/shard_map/all_gather | solution.py:54
  33.6 0.1 fusion.19
  33.7 0.5 %reduce_window_sum.21 = f32[3,5,8]{2,1,0:T(8,128)S(1)} reduce-window(f32[3,5,8]{2,1,0:T(8,128)S(1)} %get-tuple-element.2, f32[]{:T(128)} %constant.36.clone.1), window={size=1x1x8 pad=0_0x0_0x0_7}, to_apply=%region_4.5 | reduce-window | flops 840 | bytes 964 | tf_op jit(solution)/shard_map/per_device/reduce_window_sum | solution.py:60
  34.2 0.1 copy.35
  34.3 6.4 %reduce_window_sum.20 = f32[3,5,8,64]{3,2,1,0:T(8,128)S(1)} reduce-window(f32[3,5,8,64]{3,2,1,0:T(8,128)S(1)} %copy.32, f32[]{:T(128)} %constant.36.clone.1), window={size=1x1x1x64 pad=0_0x0_0x0_0x0_63}, to_apply=%region_0.1 | reduce-window | flops 483840 | bytes 61444 | tf_op jit(solution)/shard_map/per_device/reduce_window_sum | solution.py:62
  40.7 0.4 convolution_bitcast_fusion
  41.1 5.2 %all-gather.1 = f32[12,5,64]{2,1,0:T(8,128)S(1)} all-gather(f32[3,5,64]{2,1,0:T(8,128)S(1)} %convolution_bitcast_fusion), channel_id=3, replica_groups=mesh['sp'=8,'tp'=4] {'tp'}, dimensions={0}, use_global_device_ids=true | all-gather | bytes 19200 | tf_op jit(solution)/shard_map/all_gather | solution.py:70
  46.3 0.1 multiply_reduce_fusion.1
  46.4 0.1 multiply_convert_fusion
  46.5 0.7 %convert_element_type.28 = bf16[3,320]{1,0:T(4,128)(2,1)} reshape(bf16[3,5,64]{2,1,0:T(8,128)(2,1)S(1)} %multiply_convert_fusion) | data formatting | bytes 3840 | tf_op jit(solution)/shard_map/convert_element_type | solution.py:72
  47.2 0.0 copy-done.1
  (8 shorter events, 0.1 us)
Async XLA Ops:
  0.6 1.4 %copy-start = (bf16[2048,384]{1,0:T(8,128)(2,1)S(1)}, bf16[2048,384]{1,0:T(8,128)(2,1)}, u32[]{:S(2)}) copy-start(bf16[2048,384]{1,0:T(8,128)(2,1)} %param.6) | copy-start | bytes 4718596
  2.0 2.4 %copy-start.2 = (bf16[4,64,2048]{2,1,0:T(8,128)(2,1)S(1)}, bf16[4,64,2048]{2,1,0:T(8,128)(2,1)}, u32[]{:S(2)}) copy-start(bf16[4,64,2048]{2,1,0:T(8,128)(2,1)} %param.5) | copy-start | bytes 3145732
  6.9 9.1 %copy-start.4 = (f32[6,5]{1,0:T(8,128)S(1)}, f32[6,5]{1,0:T(8,128)}, u32[]{:S(2)}) copy-start(f32[6,5]{1,0:T(8,128)} %param.9) | copy-start | bytes 364
  7.6 20.2 %copy-start.3 = (bf16[3,5,64]{2,0,1:T(4,128)(2,1)S(1)}, bf16[3,5,64]{2,0,1:T(4,128)(2,1)}, u32[]{:S(2)}) copy-start(bf16[3,5,64]{2,0,1:T(4,128)(2,1)} %param.8) | copy-start | bytes 5764
  8.7 19.0 %all-to-all-start = ((bf16[24,1,64,128]{3,2,1,0:T(8,128)(2,1)}), bf16[24,1,64,128]{3,2,1,0:T(8,128)(2,1)S(1)}, u32[]{:S(2)}, u32[]{:S(2)}) async-start(bf16[24,1,64,128]{3,2,1,0:T(8,128)(2,1)} %bitcast.3), calls=%async_computation | async-start | bytes 786432 | tf_op jit(solution)/shard_map/all_to_all | solution.py:42
  27.7 19.4 %copy-start.1 = (bf16[8,3,1,64,128]{4,3,0,1,2:T(8,128)(2,1)}, bf16[8,3,1,64,128]{4,3,0,1,2:T(8,128)(2,1)S(1)}, u32[]{:S(2)}) copy-start(bf16[8,3,1,64,128]{4,3,0,1,2:T(8,128)(2,1)S(1)} %copy.51) | copy-start | bytes 1179652
